TPU v7x, 32 devices: a whole 2x2x4 slice. The times are simulated.
32 devices in a mesh: grp: 2 (over y), sp: 4 (over z), tp: 4 (over x, core).
Axes of the slice: x: 2, y: 2, z: 4, core: 2. Of those that a mesh axis runs over, the one named last changes fastest.
Arguments:
- target: bfloat16 [2048, 2048], P(('grp', 'sp', 'tp')), parts along dimension 0, may hold values from -20 to 20
- source: bfloat16 [4096, 2048], P(('grp', 'sp')), parts along dimension 0, may hold values from -20 to 20
- source_gain: float32 [2048], replicated, may hold values from 0.1 to 1.9
- query_gain: float32 [2, 2048], replicated, may hold values from 0.1 to 1.9
- out_gain: float32 [2, 2048], replicated, may hold values from 0.1 to 1.9
- query_weight: bfloat16 [2, 2048, 2048], P(None, None, 'tp'), may hold values from -1 to 1
- key_weight: bfloat16 [2, 2048, 512], P(None, None, 'tp'), may hold values from -1 to 1
- value_weight: bfloat16 [2, 2048, 512], P(None, None, 'tp'), may hold values from -0.125 to 0.125
- out_weight: bfloat16 [2, 2048, 2048], P(None, 'tp'), may hold values from -0.125 to 0.125
Outputs:
- result: bfloat16 [2048, 2048], P(('grp', 'sp', 'tp')), parts along dimension 0
There are 2 independent parts, one for each index of `grp`. A program takes and returns all parts, laid end to end along the dimension named above; an argument that names none is the same for every part. Nothing has to cross between parts.
All inputs are finite; a program needn't handle non-finite values.
Results may differ from a plain program's by a relative error of at most 0.024.
Values may be sent and summed in bfloat16 or wider, within the bound.
A program may use at most 64 MiB of HBM per device.

v0:
```python
import jax
import jax.numpy as jnp
from jax import lax
from jax.sharding import PartitionSpec as P

HD = 256
QH = 8
KVH = 2
LAYERS = 2
EPSILON = 1e-06


def swapped(value, axis, distance):
    mask = 2**distance
    pairs = [(source, source ^ mask) for source in range(lax.axis_size(axis))]
    return lax.ppermute(value, axis, pairs)


def rms_scaled(matrix_rows, gain_row):
    values = matrix_rows.astype(jnp.float32)
    inverse = lax.rsqrt(jnp.mean(values * values, axis=-1, keepdims=True) + EPSILON)
    return values * inverse * gain_row


def group_rounds(holding, bit_count, position):
    for bit_number in range(bit_count):
        my_bit = position >> bit_number & 1
        if holding.shape[0] > 1:
            halves = holding.reshape((holding.shape[0] // 2, 2) + holding.shape[1:])
            kept_part = lax.dynamic_index_in_dim(halves, my_bit, 1, False)
            outgoing = lax.dynamic_index_in_dim(halves, 1 - my_bit, 1, False)
        else:
            kept_part = holding
            outgoing = holding
        arrived = swapped(outgoing, "tp", bit_number)
        holding = jnp.where(
            my_bit == 0,
            jnp.concatenate([kept_part, arrived], 1),
            jnp.concatenate([arrived, kept_part], 1),
        )
    return holding


def spread_heads(factor, piece_index, piece_width):
    columns = jnp.repeat(factor, HD, axis=1)
    pieces = columns.reshape(factor.shape[0], columns.shape[1] // piece_width, piece_width)
    return jnp.take(pieces, piece_index, axis=1)


def merge_partials(weighted, row_peak, row_total, bit_count, position):
    piece_width = weighted.shape[2]
    piece_index = jnp.arange(weighted.shape[1], dtype=jnp.int32)
    for bit_number in range(bit_count):
        my_bit = position >> bit_number & 1
        halves = weighted.reshape(weighted.shape[0], weighted.shape[1] // 2, 2, piece_width)
        kept_part = lax.dynamic_index_in_dim(halves, my_bit, 2, False)
        outgoing = lax.dynamic_index_in_dim(halves, 1 - my_bit, 2, False)
        piece_index = lax.dynamic_index_in_dim(piece_index.reshape(-1, 2), my_bit, 1, False)
        far_weighted, far_peak, far_total = (
            swapped(outgoing.astype(jnp.bfloat16), "tp", bit_number).astype(outgoing.dtype),
            swapped(row_peak.astype(jnp.bfloat16), "tp", bit_number).astype(row_peak.dtype),
            swapped(row_total.astype(jnp.bfloat16), "tp", bit_number).astype(row_total.dtype),
        )
        new_peak = jnp.maximum(row_peak, far_peak)
        near_factor = jnp.exp(row_peak - new_peak)
        far_factor = jnp.exp(far_peak - new_peak)
        row_total = row_total * near_factor + far_total * far_factor
        weighted = kept_part * spread_heads(
            near_factor, piece_index, piece_width
        ) + far_weighted * spread_heads(far_factor, piece_index, piece_width)
        row_peak = new_peak
    return (weighted, row_total, piece_index)


def attend(carried, key_rows, value_rows, grouped, score_scale):
    row_peak, row_total, weighted = carried
    scores = (
        jnp.einsum("rhd,nd->rhn", grouped, key_rows, preferred_element_type=jnp.float32)
        * score_scale
    )
    new_peak = jnp.maximum(row_peak, jnp.max(scores, axis=2))
    weights = jnp.exp(scores - new_peak[:, :, None])
    row_total = jnp.sum(weights, axis=2)
    weighted = jnp.einsum(
        "rhn,nd->rhd", weights.astype(jnp.bfloat16), value_rows, preferred_element_type=jnp.float32
    )
    return (new_peak, row_total, weighted)


def body(
    target,
    source,
    source_gain,
    query_gain,
    out_gain,
    query_weight,
    key_weight,
    value_weight,
    out_weight,
):
    tp_devices = lax.axis_size("tp")
    group_size = tp_devices // KVH
    bit_count = group_size.bit_length() - 1
    position = lax.axis_index("tp") % group_size
    score_scale = HD ** (-0.5)
    heads_here = QH // KVH
    matrices = 2 * LAYERS
    slices = key_weight.shape[2]
    block_rows = source.shape[0] // group_size
    normed_source = rms_scaled(source, source_gain).astype(jnp.bfloat16)
    joined = jnp.concatenate(
        [
            matrix[layer_index]
            for layer_index in range(LAYERS)
            for matrix in (key_weight, value_weight)
        ],
        axis=1,
    )
    key_slices = jnp.dot(normed_source, joined, preferred_element_type=jnp.float32).astype(
        jnp.bfloat16
    )
    holding = group_rounds(
        key_slices.reshape(group_size, 1, block_rows, matrices, slices), bit_count, position
    )
    local_keys = jnp.transpose(holding[0], (2, 1, 0, 3)).reshape(matrices, block_rows, HD)
    residual = target
    stored = None
    for layer_index in range(LAYERS):
        normed = rms_scaled(residual, query_gain[layer_index]).astype(jnp.bfloat16)
        layer_weight = query_weight[layer_index]
        queries = jnp.dot(
            lax.all_gather(normed, "tp", axis=0, tiled=True),
            layer_weight,
            preferred_element_type=jnp.float32,
        ).astype(jnp.bfloat16)
        rows_all = queries.shape[0]
        gathered = group_rounds(queries[None, None], bit_count, position)[0]
        grouped = jnp.transpose(gathered, (1, 0, 2)).reshape(rows_all, heads_here, HD)
        start_state = (
            jnp.full((rows_all, heads_here), -1e30, jnp.float32),
            jnp.zeros((rows_all, heads_here), jnp.float32),
            jnp.zeros((rows_all, heads_here, HD), jnp.float32),
        )
        if layer_index == 0:
            empty_rows = jnp.zeros(
                (lax.axis_size("sp") * block_rows, matrices - 2, HD), jnp.bfloat16
            )
            later_keys = jnp.transpose(local_keys[2:], (1, 0, 2))
            updated = attend(
                (start_state + (empty_rows,))[:3],
                lax.all_gather(local_keys[0], "sp", axis=0, tiled=True),
                lax.all_gather(local_keys[1], "sp", axis=0, tiled=True),
                grouped,
                score_scale,
            )
            kept_rows = lax.all_gather(later_keys, "sp", axis=0, tiled=True)
            row_peak, row_total, weighted, stored = updated + (kept_rows,)
        else:
            row_peak, row_total, weighted = attend(
                start_state,
                stored[:, 2 * layer_index - 2],
                stored[:, 2 * layer_index - 1],
                grouped,
                score_scale,
            )
        piece_width = heads_here * HD // group_size
        merged, row_total, piece_index = merge_partials(
            weighted.reshape(rows_all, group_size, piece_width),
            row_peak,
            row_total,
            bit_count,
            position,
        )
        attended = (merged[:, 0] / spread_heads(row_total, piece_index, piece_width)[:, 0]).astype(
            jnp.bfloat16
        )
        out_layer = out_weight[layer_index]
        summed_rows = lax.psum_scatter(
            jnp.dot(attended, out_layer, preferred_element_type=jnp.float32).astype(jnp.bfloat16),
            "tp",
            scatter_dimension=0,
            tiled=True,
        ).astype(jnp.float32)
        residual = (
            residual.astype(jnp.float32) + rms_scaled(summed_rows, out_gain[layer_index])
        ).astype(jnp.bfloat16)
    return residual


def solution(mesh):
    in_specs = (
        P(("grp", "sp", "tp"), None),
        P(("grp", "sp"), None),
        P(),
        P(),
        P(),
        P(None, None, "tp"),
        P(None, None, "tp"),
        P(None, None, "tp"),
        P(None, "tp", None),
    )
    out_specs = P(("grp", "sp", "tp"), None)
    return jax.shard_map(body, mesh=mesh, in_specs=in_specs, out_specs=out_specs, check_vma=False)
```

profile of v0, /device:TPU:0, one launch (start us, length us, event | category | flops | bytes accessed | tf_op | source)
XLA Modules:
  0.0 189.7 jit_solution(303224144333175223)
XLA Ops:
  6.5 0.9 fusion.100
  7.4 1.1 fusion.51
  8.6 1.8 fusion.53
  10.4 2.7 %slice_bitcast_fusion.6 = (bf16[2048,128]{1,0:T(8,128)(2,1)S(1)}, bf16[2048,128]{1,0:T(8,128)(2,1)}, bf16[2048,128]{1,0:T(8,128)(2,1)}, bf16[2048,128]{1,0:T(8,128)(2,1)}) fusion(bf16[2,2048,128]{2,1,0:T(8,128)(2,1)} %param.18, bf16[2,2048,128]{2,1,0:T(8,128)(2,1)} %param.17), kind=kLoop, calls=%fused_computation.92 | loop fusion | bytes 4194304 | tf_op jit(solution)/shard_map/squeeze | solution.py:113
  13.2 0.5 fusion
  13.7 2.7 %fusion.36 = bf16[512,512]{1,0:T(8,128)(2,1)S(1)} fusion(bf16[2048,128]{1,0:T(8,128)(2,1)} %get-tuple-element.28, bf16[2048,128]{1,0:T(8,128)(2,1)} %get-tuple-element.41, bf16[2048,128]{1,0:T(8,128)(2,1)S(1)} %get-tuple-element.27, bf16[2048,128]{1,0:T(8,128)(2,1)} %get-tuple-element.42, bf16[512,2048]{1,0:T(8,128)(2,1)S(1)} %copy-done.1, ...), kind=kOutput, calls=%fused_computation.41 | convolution fusion | flops 1086586880 | bytes 4728832 | tf_op jit(solution)/shard_map/dot_general | solution.py:119
  16.3 0.1 reshape_reshape.27
  16.5 0.2 constant_dynamic-slice_fusion.2
  16.7 0.6 collective-permute-start.1
  17.3 1.1 collective-permute-done.1
  18.5 0.1 copy.15
  18.7 11.2 %all-gather.4.cloned.1.call-done = bf16[256,2048]{1,0:T(8,128)(2,1)} async-done(((bf16[64,2048]{1,0:T(8,128)(2,1)}), bf16[256,2048]{1,0:T(8,128)(2,1)}) %all-gather.4.cloned.1.call-update) | async-done | bytes 1048592 | tf_op jit(solution)/shard_map/all_gather | solution.py:132
  30.0 2.6 %fusion.41 = bf16[256,512]{1,0:T(8,128)(2,1)S(1)} fusion(bf16[256,2048]{1,0:T(8,128)(2,1)} %all-gather.4.cloned.1.call-done, bf16[2,2048,512]{2,1,0:T(8,128)(2,1)} %param.16), kind=kOutput, calls=%fused_computation.42 | convolution fusion | flops 537001984 | bytes 3407872 | tf_op jit(solution)/shard_map/dot_general | solution.py:131
  32.6 0.3 collective-permute-start
  32.9 16.0 %all_gather.16 = bf16[1024,256]{1,0:T(8,128)(2,1)S(1)} all-gather(bf16[256,256]{1,0:T(8,128)(2,1)S(1)} %bitcast.151), channel_id=1, replica_groups=mesh['grp'=2,'sp'=4,'tp'=4] {'sp'}, dimensions={0}, use_global_device_ids=true | all-gather | bytes 655360 | tf_op jit(solution)/shard_map/all_gather | solution.py:151
  48.9 0.1 copy.17
  49.0 16.1 %all_gather.17 = bf16[1024,256]{0,1:T(8,128)(2,1)S(1)} all-gather(bf16[256,256]{0,1:T(8,128)(2,1)S(1)} %bitcast.152), channel_id=1, replica_groups=mesh['grp'=2,'sp'=4,'tp'=4] {'sp'}, dimensions={0}, use_global_device_ids=true | all-gather | bytes 655360 | tf_op jit(solution)/shard_map/all_gather | solution.py:152
  65.2 0.2 copy.12
  65.4 0.8 multiply_reduce_fusion.1
  66.2 0.9 fusion.3
  67.2 1.0 fusion.9
  68.3 0.5 collective-permute-start.4
  68.8 0.1 collective-permute-start.2
  68.9 0.6 constant_dynamic-slice_fusion
  71.7 1.9 convolution_convert_fusion.1
  73.7 24.6 %reduce-scatter.3.cloned.1.call-done = bf16[64,2048]{1,0:T(8,128)(2,1)} async-done(((bf16[256,2048]{1,0:T(8,128)(2,1)}), bf16[64,2048]{1,0:T(8,128)(2,1)}) %reduce-scatter.3.cloned.1.call-update) | async-done | bytes 262160 | tf_op jit(solution)/shard_map/reduce_scatter | solution.py:178
  98.3 1.1 fusion.47
  99.5 1.2 fusion.55
  100.7 0.8 fusion.57
  101.7 0.7 bitcast_bitcast_fusion
  102.4 0.2 reduce-scatter.5.cloned.1.call-start
  102.7 15.8 %all-gather.6.cloned.1.call-done = bf16[256,2048]{1,0:T(8,128)(2,1)} async-done(((bf16[64,2048]{1,0:T(8,128)(2,1)}), bf16[256,2048]{1,0:T(8,128)(2,1)}) %all-gather.6.cloned.1.call-update) | async-done | bytes 1048592 | tf_op jit(solution)/shard_map/all_gather | solution.py:132
  118.5 2.6 %fusion.44 = bf16[256,512]{1,0:T(8,128)(2,1)S(1)} fusion(bf16[256,2048]{1,0:T(8,128)(2,1)} %all-gather.6.cloned.1.call-done, bf16[2,2048,512]{2,1,0:T(8,128)(2,1)} %param.16), kind=kOutput, calls=%fused_computation.43 | convolution fusion | flops 537001984 | bytes 3407872 | tf_op jit(solution)/shard_map/dot_general | solution.py:131
  121.1 0.3 collective-permute-start.5
  121.4 1.3 collective-permute-done.5
  122.8 0.2 copy.18
  123.0 24.9 %all-gather.8.cloned.1.call-done = bf16[1024,2,256]{2,0,1:T(8,128)(2,1)} async-done(((bf16[256,2,256]{2,0,1:T(8,128)(2,1)}), bf16[1024,2,256]{2,0,1:T(8,128)(2,1)}) %all-gather.8.cloned.1.call-update) | async-done | bytes 1048592 | tf_op jit(solution)/shard_map/all_gather | solution.py:156
  147.9 2.0 %multiply_reduce_fusion = (f32[256,4]{0,1:T(4,128)S(1)}, f32[256,4,1024]{2,0,1:T(8,128)S(1)}) fusion(bf16[256,4,256]{0,2,1:T(8,128)(2,1)S(1)} %bitcast.138, bf16[1024,2,256]{2,0,1:T(8,128)(2,1)} %all-gather.8.cloned.1.call-done), kind=kOutput, calls=%fused_computation.7 | convolution fusion | flops 538967040 | bytes 5246976 | tf_op jit(solution)/shard_map/rhd,nd->rhn/dot_general | solution.py:78
  149.9 0.9 fusion.5
  150.8 1.1 fusion.7
  152.1 0.5 collective-permute-start.8
  152.6 0.1 collective-permute-start.6
  152.7 0.9 collective-permute-done.8
  153.6 0.1 collective-permute-done.6
  154.0 1.8 convolution_convert_fusion
  155.9 24.3 %reduce-scatter.5.cloned.1.call-done = bf16[64,2048]{1,0:T(8,128)(2,1)} async-done(((bf16[256,2048]{1,0:T(8,128)(2,1)}), bf16[64,2048]{1,0:T(8,128)(2,1)}) %reduce-scatter.5.cloned.1.call-update) | async-done | bytes 262160 | tf_op jit(solution)/shard_map/reduce_scatter | solution.py:178
  180.2 1.1 fusion.49
  181.3 1.8 fusion.58
  (60 shorter events, 1.3 us)
Async XLA Ops:
  6.5 6.6 %copy-start.1 = (bf16[512,2048]{1,0:T(8,128)(2,1)S(1)}, bf16[512,2048]{1,0:T(8,128)(2,1)}, u32[]{:S(2)}) copy-start(bf16[512,2048]{1,0:T(8,128)(2,1)} %param.12) | copy-start | bytes 6291460
  6.5 7.1 %copy-start.6 = (f32[2048]{0:T(1024)S(1)}, f32[2048]{0:T(1024)}, u32[]{:S(2)}) copy-start(f32[2048]{0:T(1024)} %param.13) | copy-start | bytes 24580
  6.5 23.4 %all-gather.4.cloned.1.call-start = ((), (), s32[]{:S(2)}) async-start(), calls=%async_computation.2 | async-start | bytes 1310720 | tf_op jit(solution)/shard_map/all_gather | solution.py:132
  10.4 88.0 %reduce-scatter.3.cloned.1.call-start = ((), (), s32[]{:S(2)}) async-start(), calls=%async_computation.3 | async-start | bytes 1310720 | tf_op jit(solution)/shard_map/reduce_scatter | solution.py:178
  16.7 1.7 collective-permute-start.1
  32.6 32.5 %collective-permute-start = (bf16[1,1,256,512]{3,2,1,0:T(8,128)(2,1)S(1)}, bf16[1,1,256,512]{3,2,1,0:T(8,128)(2,1)S(1)}, u32[]{:S(2)}, u32[]{:S(2)}) collective-permute-start(bf16[1,1,256,512]{3,2,1,0:T(8,128)(2,1)S(1)} %bitcast.155), channel_id=1, source_target_pairs={{0,1},{1,0},{2,3},{3,2},{4,5},{5,4},{6,7},{7,6},{8,9},{9,8},{10,11... | collective-permute-start | bytes 786440 | tf_op jit(solution)/shard_map/ppermute | solution.py:16
  67.2 4.6 %copy-start.4 = (bf16[2,512,2048]{2,1,0:T(8,128)(2,1)S(1)}, bf16[2,512,2048]{2,1,0:T(8,128)(2,1)}, u32[]{:S(2)}) copy-start(bf16[2,512,2048]{2,1,0:T(8,128)(2,1)} %param.19) | copy-start | bytes 12582916
  68.2 3.3 %collective-permute-start.3 = (bf16[256,1,512]{0,2,1:T(8,128)(2,1)S(1)}, bf16[256,1,512]{0,2,1:T(8,128)(2,1)S(1)}, u32[]{:S(2)}, u32[]{:S(2)}) collective-permute-start(bf16[256,1,512]{0,2,1:T(8,128)(2,1)S(1)} %fusion.72), channel_id=1, source_target_pairs={{0,1},{1,0},{2,3},{3,2},{4,5},{5,4},{6,7},{7,6},{8,9},{9,8},{10,11... | collective-permute-start | bytes 786440 | tf_op jit(solution)/shard_map/ppermute | solution.py:16
  68.3 3.1 %collective-permute-start.4 = (bf16[256,4]{0,1:T(4,128)(2,1)S(1)}, bf16[256,4]{0,1:T(4,128)(2,1)S(1)}, u32[]{:S(2)}, u32[]{:S(2)}) collective-permute-start(bf16[256,4]{0,1:T(4,128)(2,1)S(1)} %convert_element_type.135), channel_id=1, source_target_pairs={{0,1},{1,0},{2,3},{3,2},{4,5},{5,4},{6,7},{7,6},{8,9},{9,8},{10,11... | collective-permute-start | bytes 6152 | tf_op jit(solution)/shard_map/ppermute | solution.py:16
  68.8 2.6 %collective-permute-start.2 = (bf16[256,4]{0,1:T(4,128)(2,1)S(1)}, bf16[256,4]{0,1:T(4,128)(2,1)S(1)}, u32[]{:S(2)}, u32[]{:S(2)}) collective-permute-start(bf16[256,4]{0,1:T(4,128)(2,1)S(1)} %fusion.91), channel_id=1, source_target_pairs={{0,1},{1,0},{2,3},{3,2},{4,5},{5,4},{6,7},{7,6},{8,9},{9,8},{10,11... | collective-permute-start | bytes 6152 | tf_op jit(solution)/shard_map/ppermute | solution.py:16
  71.6 2.0 %copy-start.3 = (f32[2,2048]{1,0:T(2,128)S(1)}, f32[2,2048]{1,0:T(2,128)}, u32[]{:S(2)}) copy-start(f32[2,2048]{1,0:T(2,128)} %param.15) | copy-start | bytes 49156
  71.6 27.8 %copy-start = (bf16[64,2048]{1,0:T(8,128)(2,1)S(1)}, bf16[64,2048]{1,0:T(8,128)(2,1)}, u32[]{:S(2)}) copy-start(bf16[64,2048]{1,0:T(8,128)(2,1)} %param.11) | copy-start | bytes 786436
  73.6 44.8 %all-gather.6.cloned.1.call-start = ((), (), s32[]{:S(2)}) async-start(), calls=%async_computation.4 | async-start | bytes 1310720 | tf_op jit(solution)/shard_map/all_gather | solution.py:132
  101.6 46.3 %all-gather.8.cloned.1.call-start = ((), (), s32[]{:S(2)}) async-start(), calls=%async_computation.5 | async-start | bytes 1310720 | tf_op jit(solution)/shard_map/all_gather | solution.py:156
  102.4 77.8 %reduce-scatter.5.cloned.1.call-start = ((), (), s32[]{:S(2)}) async-start(), calls=%async_computation.6 | async-start | bytes 1310720 | tf_op jit(solution)/shard_map/reduce_scatter | solution.py:178
  121.1 1.6 collective-permute-start.5
  147.9 2.9 %copy-start.2 = (bf16[1024,2,256]{2,0,1:T(8,128)(2,1)S(1)}, bf16[1024,2,256]{2,0,1:T(8,128)(2,1)}, u32[]{:S(2)}) copy-start(bf16[1024,2,256]{2,0,1:T(8,128)(2,1)} %all-gather.8.cloned.1.call-done) | copy-start | bytes 3145732
  150.8 3.2 %copy-start.5 = (bf16[2,512,2048]{2,1,0:T(8,128)(2,1)S(1)}, bf16[2,512,2048]{2,1,0:T(8,128)(2,1)}, u32[]{:S(2)}) copy-start(bf16[2,512,2048]{2,1,0:T(8,128)(2,1)} %param.19) | copy-start | bytes 12582916
  152.0 1.8 collective-permute-start.7
  152.1 1.5 collective-permute-start.8
  152.6 1.2 collective-permute-start.6
Sparse Core Ops, SparseCore 0:
  10.5 19.4 all-gather.3
  73.7 24.5 reduce-scatter.2
  101.7 16.6 all-gather.5
  119.9 27.9 all-gather.7
  156.0 24.1 reduce-scatter.4
where the time goes:
time: 190 us
  waiting for transfers between devices  105 us (55%)
  blocking collectives  32.1 us (17%)
  matrix products  16.5 us (9%)
  between operations  15.5 us (8%)
  other arithmetic  11.6 us (6%)
  local copies, waits for them, and re-layouts  6.59 us (3%)
  starting transfers between devices  2.78 us (1%)
    reduce_scatter x2, waiting for transfers between devices, body(): lax.psum_scatter(jnp.dot(attended, out_layer, preferred_element_type=jnp....  49 us
    all_gather x2, waiting for transfers between devices, body(): lax.all_gather(normed, 'tp', axis=0, tiled=True)  27 us
    all_gather x1, waiting for transfers between devices, body(): kept_rows = lax.all_gather(later_keys, 'sp', axis=0, tiled=True)  24.9 us
    all_gather x1, blocking collectives, body(): lax.all_gather(local_keys[1], 'sp', axis=0, tiled=True)  16.1 us
    all_gather x1, blocking collectives, body(): lax.all_gather(local_keys[0], 'sp', axis=0, tiled=True)  16 us
    dot_general x2, matrix products, body(): jnp.dot(lax.all_gather(normed, 'tp', axis=0, tiled=True), layer_weight, p...  5.24 us
    reduce_sum x5, other arithmetic, rms_scaled(): jnp.mean(values * values, axis=-1, keepdims=True) + EPSILON  5.04 us
  transfers between devices with their start and end apart: 14, of which 9 were waited for; matrix products, arithmetic and copies ran while one was open for 6% of the time, Pallas kernels for 0%

commit v1 on v0

--- a/solution.py
+++ b/solution.py
@@ -153,7 +153,14 @@
                 grouped,
                 score_scale,
             )
-            kept_rows = lax.all_gather(later_keys, "sp", axis=0, tiled=True)
+            size = lax.axis_size("sp")
+            right = [(i, (i + 1) % size) for i in range(size)]
+            parts = [later_keys]
+            for far in range(1, size):
+                parts = [lax.ppermute(parts[0], "sp", right), *parts]
+            out = jnp.concatenate(parts, axis=0)
+            shift = (lax.axis_index("sp") + 1) * parts[-1].shape[0]
+            kept_rows = jnp.roll(out, shift, axis=0)
             row_peak, row_total, weighted, stored = updated + (kept_rows,)
         else:
             row_peak, row_total, weighted = attend(

time: 190 us -> 170 us (0.89)
  waiting for transfers between devices: 105 us -> 76 us
  local copies, waits for them, and re-layouts: 6.59 us -> 11.6 us
  starting transfers between devices: 2.78 us -> 5.35 us
    all_gather x1 -> x0, waiting for transfers between devices: 24.9 us -> none  [body(): kept_rows = lax.all_gather(later_keys, 'sp', axis=0, tiled=True)]
    ppermute x0 -> x3, waiting for transfers between devices: none -> 17 us  [body(): parts = [lax.ppermute(parts[0], 'sp', right), *parts]]
    all_gather x2, waiting for transfers between devices: 27 us -> 11.2 us  [body(): lax.all_gather(normed, 'tp', axis=0, tiled=True)]
    unnamed x17 -> x22, local copies, waits for them, and re-layouts: 0.13 us -> 5.16 us
    reduce_scatter x2, waiting for transfers between devices: 49 us -> 45.6 us  [body(): lax.psum_scatter(jnp.dot(attended, out_layer, preferred_element_type=jnp....]
    ppermute x0 -> x3, starting transfers between devices: none -> 2.65 us  [body(): parts = [lax.ppermute(parts[0], 'sp', right), *parts]]
  transfers between devices with their start and end apart: 14 -> 16, of which waited for: 9 -> 9; matrix products, arithmetic and copies ran while one was open for 6% -> 10% of each run, Pallas kernels for 0% -> 0%
where the time goes in v1:
time: 170 us
  waiting for transfers between devices  76 us (45%)
  blocking collectives  32.1 us (19%)
  matrix products  17.6 us (10%)
  between operations  15.5 us (9%)
  local copies, waits for them, and re-layouts  11.6 us (7%)
  other arithmetic  11.6 us (7%)
  starting transfers between devices  5.35 us (3%)
    reduce_scatter x2, waiting for transfers between devices, body(): lax.psum_scatter(jnp.dot(attended, out_layer, preferred_element_type=jnp....  45.6 us
    ppermute x3, waiting for transfers between devices, body(): parts = [lax.ppermute(parts[0], 'sp', right), *parts]  17 us
    all_gather x1, blocking collectives, body(): lax.all_gather(local_keys[1], 'sp', axis=0, tiled=True)  16.1 us
    all_gather x1, blocking collectives, body(): lax.all_gather(local_keys[0], 'sp', axis=0, tiled=True)  16 us
    all_gather x2, waiting for transfers between devices, body(): lax.all_gather(normed, 'tp', axis=0, tiled=True)  11.2 us
    dot_general x2, matrix products, body(): jnp.dot(lax.all_gather(normed, 'tp', axis=0, tiled=True), layer_weight, p...  5.24 us
    unnamed x22, local copies, waits for them, and re-layouts  5.16 us
    reduce_sum x5, other arithmetic, rms_scaled(): jnp.mean(values * values, axis=-1, keepdims=True) + EPSILON  5.04 us
  transfers between devices with their start and end apart: 16, of which 9 were waited for; matrix products, arithmetic and copies ran while one was open for 10% of the time, Pallas kernels for 0%

profile of v1, /device:TPU:0, one launch (start us, length us, event | category | flops | bytes accessed | tf_op | source)
XLA Modules:
  0.0 169.8 jit_solution(168338487816612429)
XLA Ops:
  6.5 0.9 fusion.102
  7.4 1.1 fusion.51
  8.6 1.8 %fusion.53 = bf16[64,2048]{1,0:T(8,128)(2,1)} fusion(bf16[64,2048]{1,0:T(8,128)(2,1)} %param.11, f32[2048]{0:T(1024)S(1)} %bitcast.175, f32[64]{0:T(128)S(1)} %add_rsqrt_fusion.4), kind=kLoop, calls=%fused_computation.60 | loop fusion | flops 524288 | bytes 532736 | tf_op jit(solution)/shard_map/convert_element_type | solution.py:129
  10.4 2.7 %slice_bitcast_fusion.2 = (bf16[2048,128]{1,0:T(8,128)(2,1)S(1)}, bf16[2048,128]{1,0:T(8,128)(2,1)}, bf16[2048,128]{1,0:T(8,128)(2,1)}, bf16[2048,128]{1,0:T(8,128)(2,1)}) fusion(bf16[2,2048,128]{2,1,0:T(8,128)(2,1)} %param.18, bf16[2,2048,128]{2,1,0:T(8,128)(2,1)} %param.17), kind=kLoop, calls=%fused_computation.92 | loop fusion | bytes 4194304 | tf_op jit(solution)/shard_map/squeeze | solution.py:113
  13.2 0.5 fusion
  13.7 2.7 %fusion.36 = bf16[512,512]{1,0:T(8,128)(2,1)S(1)} fusion(bf16[2048,128]{1,0:T(8,128)(2,1)} %get-tuple-element.28, bf16[2048,128]{1,0:T(8,128)(2,1)} %get-tuple-element.41, bf16[2048,128]{1,0:T(8,128)(2,1)S(1)} %get-tuple-element.27, bf16[2048,128]{1,0:T(8,128)(2,1)} %get-tuple-element.42, bf16[512,2048]{1,0:T(8,128)(2,1)S(1)} %copy-done.1, ...), kind=kOutput, calls=%fused_computation.41 | convolution fusion | flops 1086586880 | bytes 4728832 | tf_op jit(solution)/shard_map/dot_general | solution.py:119
  16.7 0.6 collective-permute-start.1
  17.3 1.1 collective-permute-done.1
  18.7 11.2 %all-gather.3.cloned.1.call-done = bf16[256,2048]{1,0:T(8,128)(2,1)} async-done(((bf16[64,2048]{1,0:T(8,128)(2,1)}), bf16[256,2048]{1,0:T(8,128)(2,1)}) %all-gather.3.cloned.1.call-update) | async-done | bytes 1048592 | tf_op jit(solution)/shard_map/all_gather | solution.py:132
  30.0 2.6 %fusion.41 = bf16[256,512]{1,0:T(8,128)(2,1)S(1)} fusion(bf16[256,2048]{1,0:T(8,128)(2,1)} %all-gather.3.cloned.1.call-done, bf16[2,2048,512]{2,1,0:T(8,128)(2,1)} %param.16), kind=kOutput, calls=%fused_computation.42 | convolution fusion | flops 537001984 | bytes 3407872 | tf_op jit(solution)/shard_map/dot_general | solution.py:131
  32.6 0.3 collective-permute-start
  32.9 16.0 %all_gather.13 = bf16[1024,256]{1,0:T(8,128)(2,1)S(1)} all-gather(bf16[256,256]{1,0:T(8,128)(2,1)S(1)} %bitcast.161), channel_id=1, replica_groups=mesh['grp'=2,'sp'=4,'tp'=4] {'sp'}, dimensions={0}, use_global_device_ids=true | all-gather | bytes 655360 | tf_op jit(solution)/shard_map/all_gather | solution.py:151
  49.0 16.1 %all_gather.14 = bf16[1024,256]{0,1:T(8,128)(2,1)S(1)} all-gather(bf16[256,256]{0,1:T(8,128)(2,1)S(1)} %bitcast.162), channel_id=1, replica_groups=mesh['grp'=2,'sp'=4,'tp'=4] {'sp'}, dimensions={0}, use_global_device_ids=true | all-gather | bytes 655360 | tf_op jit(solution)/shard_map/all_gather | solution.py:152
  65.2 0.2 copy.12
  65.4 0.8 multiply_reduce_fusion.1
  66.2 0.9 fusion.3
  67.2 1.0 fusion.9
  68.3 0.5 collective-permute-start.4
  68.9 0.6 constant_dynamic-slice_fusion
  71.7 1.8 %convolution_convert_fusion.1 = bf16[256,2048]{1,0:T(8,128)(2,1)} fusion(bf16[2,512,2048]{2,1,0:T(8,128)(2,1)S(1)} %copy-done.3, f32[256,2,512]{0,2,1:T(8,128)S(1)} %bitcast.159, s32[]{:T(128)} %bitcast.23, f32[256,2,512]{0,2,1:T(8,128)S(1)} %bitcast.158, f32[256,2,512]{0,2,1:T(8,128)S(1)} %bitcast.156, ...), kind=kOutput, calls=%fused_computation.14 | convolution fusion | flops 538574848 | bytes 5505033 | tf_op jit(solution)/shard_map/dot_general | solution.py:186
  73.7 1.1 collective-permute-start.6
  74.8 23.5 %reduce-scatter.3.cloned.1.call-done = bf16[64,2048]{1,0:T(8,128)(2,1)} async-done(((bf16[256,2048]{1,0:T(8,128)(2,1)}), bf16[64,2048]{1,0:T(8,128)(2,1)}) %reduce-scatter.3.cloned.1.call-update) | async-done | bytes 262160 | tf_op jit(solution)/shard_map/reduce_scatter | solution.py:185
  98.3 1.1 fusion.47
  99.4 1.3 fusion.55
  100.7 0.8 fusion.57
  101.6 1.5 collective-permute-start.7
  103.2 8.2 %collective-permute-done.7 = bf16[256,2,256]{2,0,1:T(8,128)(2,1)S(1)} collective-permute-done((bf16[256,2,256]{2,0,1:T(8,128)(2,1)S(1)}, bf16[256,2,256]{2,0,1:T(8,128)(2,1)S(1)}, u32[]{:S(2)}, u32[]{:S(2)}) %collective-permute-start.7) | collective-permute-done | bytes 262176 | tf_op jit(solution)/shard_map/ppermute | solution.py:160
  111.4 8.8 %collective-permute-done.8 = bf16[256,2,256]{2,0,1:T(8,128)(2,1)S(1)} collective-permute-done((bf16[256,2,256]{2,0,1:T(8,128)(2,1)S(1)}, bf16[256,2,256]{2,0,1:T(8,128)(2,1)S(1)}, u32[]{:S(2)}, u32[]{:S(2)}) %collective-permute-start.8) | collective-permute-done | bytes 262176 | tf_op jit(solution)/shard_map/ppermute | solution.py:160
  120.2 0.7 constant_dynamic-update-slice_fusion.7
  121.0 0.7 constant_dynamic-update-slice_fusion.6
  121.7 0.7 constant_dynamic-update-slice_fusion.5
  122.4 0.7 constant_dynamic-update-slice_fusion.4
  123.1 0.7 constant_dynamic-update-slice_fusion.3
  123.8 0.7 constant_dynamic-update-slice_fusion.2
  124.5 2.6 %fusion.44 = bf16[256,512]{1,0:T(8,128)(2,1)S(1)} fusion(bf16[256,2048]{1,0:T(8,128)(2,1)} %all-gather.5.cloned.1.call-done, bf16[2,2048,512]{2,1,0:T(8,128)(2,1)} %param.16), kind=kOutput, calls=%fused_computation.43 | convolution fusion | flops 537001984 | bytes 3407872 | tf_op jit(solution)/shard_map/dot_general | solution.py:131
  127.2 0.7 constant_dynamic-update-slice_fusion.1
  128.0 0.7 constant_dynamic-update-slice_fusion
  128.8 0.2 copy.18
  129.1 1.9 %multiply_reduce_fusion = (f32[256,4]{0,1:T(4,128)S(1)}, f32[256,4,1024]{2,0,1:T(8,128)S(1)}) fusion(bf16[256,4,256]{0,2,1:T(8,128)(2,1)S(1)} %bitcast.149, bf16[2048,2,256]{2,0,1:T(8,128)(2,1)} %constant_dynamic-update-slice_fusion, s32[]{:T(128)S(6)} %select_n.87), kind=kOutput, calls=%fused_computation.7 | convolution fusion | flops 538967040 | bytes 5246980 | tf_op jit(solution)/shard_map/rhd,nd->rhn/dot_general | solution.py:78
  130.9 0.9 fusion.5
  131.9 2.3 %fusion.7 = f32[256,4,256]{0,2,1:T(8,128)S(1)} fusion(f32[256,4,1024]{2,0,1:T(8,128)S(1)} %get-tuple-element.40, f32[256,4]{0,1:T(4,128)S(1)} %broadcast_maximum_fusion, bf16[2048,2,256]{2,0,1:T(8,128)(2,1)} %constant_dynamic-update-slice_fusion, s32[]{:T(128)S(6)} %select_n.87, s32[]{:T(128)S(6)} %add.132), kind=kOutput, calls=%fused_computation.15 | convolution fusion | flops 540016640 | bytes 5771272 | tf_op jit(solution)/shard_map/rhn,nd->rhd/dot_general | solution.py:84
  134.2 0.5 collective-permute-start.10
  134.8 0.4 collective-permute-start.9
  135.2 0.7 collective-permute-done.11
  136.3 1.8 %convolution_convert_fusion = bf16[256,2048]{1,0:T(8,128)(2,1)} fusion(bf16[2,512,2048]{2,1,0:T(8,128)(2,1)S(1)} %copy-done.4, f32[256,2,512]{0,2,1:T(8,128)S(1)} %bitcast.157, s32[]{:T(128)} %bitcast.23, f32[256,2,512]{0,2,1:T(8,128)S(1)} %bitcast.155, f32[256,2,512]{0,2,1:T(8,128)S(1)} %bitcast.154, bf16[256,1,512]{0,2,1:T(8,128)(2,1)S(1)} %collective-permute-done.10, ...), kind=kOutput, calls=%fused_computation.13 | convolution fusion | flops 538574848 | bytes 5505033 | tf_op jit(solution)/shard_map/dot_general | solution.py:186
  138.2 22.2 %reduce-scatter.5.cloned.1.call-done = bf16[64,2048]{1,0:T(8,128)(2,1)} async-done(((bf16[256,2048]{1,0:T(8,128)(2,1)}), bf16[64,2048]{1,0:T(8,128)(2,1)}) %reduce-scatter.5.cloned.1.call-update) | async-done | bytes 262160 | tf_op jit(solution)/shard_map/reduce_scatter | solution.py:185
  160.4 1.1 fusion.49
  161.5 1.8 %fusion.58 = bf16[64,2048]{1,0:T(8,128)(2,1)} fusion(bf16[64,2048]{1,0:T(8,128)(2,1)} %reduce-scatter.5.cloned.1.call-done, bf16[64,2048]{1,0:T(8,128)(2,1)S(1)} %get-tuple-element.21, f32[2048]{0:T(1024)S(1)} %bitcast.173, f32[64]{0:T(128)S(1)} %add_rsqrt_fusion.1), kind=kLoop, calls=%fused_computation.65 | loop fusion | flops 786432 | bytes 794880 | tf_op jit(solution)/shard_map/convert_element_type | solution.py:193
  (69 shorter events, 2.4 us)
Async XLA Ops:
  6.5 6.6 %copy-start.1 = (bf16[512,2048]{1,0:T(8,128)(2,1)S(1)}, bf16[512,2048]{1,0:T(8,128)(2,1)}, u32[]{:S(2)}) copy-start(bf16[512,2048]{1,0:T(8,128)(2,1)} %param.12) | copy-start | bytes 6291460
  6.5 7.2 %copy-start.5 = (f32[2048]{0:T(1024)S(1)}, f32[2048]{0:T(1024)}, u32[]{:S(2)}) copy-start(f32[2048]{0:T(1024)} %param.13) | copy-start | bytes 24580
  6.5 23.4 %all-gather.3.cloned.1.call-start = ((), (), s32[]{:S(2)}) async-start(), calls=%async_computation.2 | async-start | bytes 1310720 | tf_op jit(solution)/shard_map/all_gather | solution.py:132
  10.4 87.9 %reduce-scatter.3.cloned.1.call-start = ((), (), s32[]{:S(2)}) async-start(), calls=%async_computation.3 | async-start | bytes 1310720 | tf_op jit(solution)/shard_map/reduce_scatter | solution.py:185
  16.7 1.7 %collective-permute-start.1 = (bf16[1,1,256,4,128]{4,2,3,1,0:T(8,128)(2,1)S(1)}, bf16[1,1,256,4,128]{4,2,3,1,0:T(8,128)(2,1)S(1)}, u32[]{:S(2)}, u32[]{:S(2)}) collective-permute-start(bf16[1,1,256,4,128]{4,2,3,1,0:T(8,128)(2,1)S(1)} %bitcast.164), channel_id=1, source_target_pairs={{0,1},{1,0},{2,3},{3,2},{4,5},{5,4},{6,7},{7,6},{8,9},{9,8},{10,11... | collective-permute-start | bytes 786440 | tf_op jit(solution)/shard_map/ppermute | solution.py:16
  32.6 32.5 %collective-permute-start = (bf16[1,1,256,512]{3,2,1,0:T(8,128)(2,1)S(1)}, bf16[1,1,256,512]{3,2,1,0:T(8,128)(2,1)S(1)}, u32[]{:S(2)}, u32[]{:S(2)}) collective-permute-start(bf16[1,1,256,512]{3,2,1,0:T(8,128)(2,1)S(1)} %bitcast.165), channel_id=1, source_target_pairs={{0,1},{1,0},{2,3},{3,2},{4,5},{5,4},{6,7},{7,6},{8,9},{9,8},{10,11... | collective-permute-start | bytes 786440 | tf_op jit(solution)/shard_map/ppermute | solution.py:16
  67.2 4.6 %copy-start.3 = (bf16[2,512,2048]{2,1,0:T(8,128)(2,1)S(1)}, bf16[2,512,2048]{2,1,0:T(8,128)(2,1)}, u32[]{:S(2)}) copy-start(bf16[2,512,2048]{2,1,0:T(8,128)(2,1)} %param.19) | copy-start | bytes 12582916
  68.2 3.3 %collective-permute-start.3 = (bf16[256,1,512]{0,2,1:T(8,128)(2,1)S(1)}, bf16[256,1,512]{0,2,1:T(8,128)(2,1)S(1)}, u32[]{:S(2)}, u32[]{:S(2)}) collective-permute-start(bf16[256,1,512]{0,2,1:T(8,128)(2,1)S(1)} %fusion.72), channel_id=1, source_target_pairs={{0,1},{1,0},{2,3},{3,2},{4,5},{5,4},{6,7},{7,6},{8,9},{9,8},{10,11... | collective-permute-start | bytes 786440 | tf_op jit(solution)/shard_map/ppermute | solution.py:16
  68.3 3.1 %collective-permute-start.4 = (bf16[256,4]{0,1:T(4,128)(2,1)S(1)}, bf16[256,4]{0,1:T(4,128)(2,1)S(1)}, u32[]{:S(2)}, u32[]{:S(2)}) collective-permute-start(bf16[256,4]{0,1:T(4,128)(2,1)S(1)} %convert_element_type.135), channel_id=1, source_target_pairs={{0,1},{1,0},{2,3},{3,2},{4,5},{5,4},{6,7},{7,6},{8,9},{9,8},{10,11... | collective-permute-start | bytes 6152 | tf_op jit(solution)/shard_map/ppermute | solution.py:16
  68.8 2.6 %collective-permute-start.2 = (bf16[256,4]{0,1:T(4,128)(2,1)S(1)}, bf16[256,4]{0,1:T(4,128)(2,1)S(1)}, u32[]{:S(2)}, u32[]{:S(2)}) collective-permute-start(bf16[256,4]{0,1:T(4,128)(2,1)S(1)} %fusion.93), channel_id=1, source_target_pairs={{0,1},{1,0},{2,3},{3,2},{4,5},{5,4},{6,7},{7,6},{8,9},{9,8},{10,11... | collective-permute-start | bytes 6152 | tf_op jit(solution)/shard_map/ppermute | solution.py:16
  71.6 2.0 %copy-start.2 = (f32[2,2048]{1,0:T(2,128)S(1)}, f32[2,2048]{1,0:T(2,128)}, u32[]{:S(2)}) copy-start(f32[2,2048]{1,0:T(2,128)} %param.15) | copy-start | bytes 49156
  71.7 27.7 %copy-start = (bf16[64,2048]{1,0:T(8,128)(2,1)S(1)}, bf16[64,2048]{1,0:T(8,128)(2,1)}, u32[]{:S(2)}) copy-start(bf16[64,2048]{1,0:T(8,128)(2,1)} %param.11) | copy-start | bytes 786436
  73.6 50.9 %all-gather.5.cloned.1.call-start = ((), (), s32[]{:S(2)}) async-start(), calls=%async_computation.4 | async-start | bytes 1310720 | tf_op jit(solution)/shard_map/all_gather | solution.py:132
  73.7 27.9 %collective-permute-start.6 = (bf16[256,2,256]{2,0,1:T(8,128)(2,1)S(1)}, bf16[256,2,256]{2,0,1:T(8,128)(2,1)S(1)}, u32[]{:S(2)}, u32[]{:S(2)}) collective-permute-start(bf16[256,2,256]{2,0,1:T(8,128)(2,1)S(1)} %bitcast_bitcast_fusion), channel_id=1, source_target_pairs={{0,4},{4,8},{8,12},{12,0},{1,5},{5,9},{9,13},{13,1},{2,6},{6,10},{... | collective-permute-start | bytes 786440 | tf_op jit(solution)/shard_map/ppermute | solution.py:160
  101.6 58.8 %reduce-scatter.5.cloned.1.call-start = ((), (), s32[]{:S(2)}) async-start(), calls=%async_computation.5 | async-start | bytes 1310720 | tf_op jit(solution)/shard_map/reduce_scatter | solution.py:185
  101.6 9.8 %collective-permute-start.7 = (bf16[256,2,256]{2,0,1:T(8,128)(2,1)S(1)}, bf16[256,2,256]{2,0,1:T(8,128)(2,1)S(1)}, u32[]{:S(2)}, u32[]{:S(2)}) collective-permute-start(bf16[256,2,256]{2,0,1:T(8,128)(2,1)S(1)} %collective-permute-done.6), channel_id=1, source_target_pairs={{0,4},{4,8},{8,12},{12,0},{1,5},{5,9},{9,13},{13,1},{2,6},{6,10},{... | collective-permute-start | bytes 786440 | tf_op jit(solution)/shard_map/ppermute | solution.py:160
  111.4 8.8 %collective-permute-start.8 = (bf16[256,2,256]{2,0,1:T(8,128)(2,1)S(1)}, bf16[256,2,256]{2,0,1:T(8,128)(2,1)S(1)}, u32[]{:S(2)}, u32[]{:S(2)}) collective-permute-start(bf16[256,2,256]{2,0,1:T(8,128)(2,1)S(1)} %collective-permute-done.7), channel_id=1, source_target_pairs={{0,4},{4,8},{8,12},{12,0},{1,5},{5,9},{9,13},{13,1},{2,6},{6,10},{... | collective-permute-start | bytes 786440 | tf_op jit(solution)/shard_map/ppermute | solution.py:160
  127.2 1.6 collective-permute-start.5
  131.9 4.5 %copy-start.4 = (bf16[2,512,2048]{2,1,0:T(8,128)(2,1)S(1)}, bf16[2,512,2048]{2,1,0:T(8,128)(2,1)}, u32[]{:S(2)}) copy-start(bf16[2,512,2048]{2,1,0:T(8,128)(2,1)} %param.19) | copy-start | bytes 12582916
  134.2 1.9 %collective-permute-start.10 = (bf16[256,1,512]{0,2,1:T(8,128)(2,1)S(1)}, bf16[256,1,512]{0,2,1:T(8,128)(2,1)S(1)}, u32[]{:S(2)}, u32[]{:S(2)}) collective-permute-start(bf16[256,1,512]{0,2,1:T(8,128)(2,1)S(1)} %fusion.73), channel_id=1, source_target_pairs={{0,1},{1,0},{2,3},{3,2},{4,5},{5,4},{6,7},{7,6},{8,9},{9,8},{10,11... | collective-permute-start | bytes 786440 | tf_op jit(solution)/shard_map/ppermute | solution.py:16
  134.7 1.2 collective-permute-start.11
  134.8 1.2 collective-permute-start.9
Sparse Core Ops, SparseCore 0:
  10.5 19.4 all-gather.2
  73.7 24.5 reduce-scatter.2
  101.7 16.6 all-gather.4
  138.3 22.0 reduce-scatter.4
